TPU v7x, 512 devices: a whole 4x4x16 slice. The times are simulated.
512 devices in a mesh: sp: 64 (over z, y), tp: 8 (over x, core).
Axes of the slice: x: 4, y: 4, z: 16, core: 2. Of those that a mesh axis runs over, the one named last changes fastest.
Arguments:
- residual: bfloat16 [16384, 2048], P('sp'), may hold values from -6 to 6
- queries: bfloat16 [16384, 1024], P('sp', 'tp'), may hold values from -6 to 6
- forget_gate_logits: bfloat16 [16384, 1024], P('sp', 'tp'), may hold values from -5 to 5
- projected_values: bfloat16 [16384, 1024], P('sp', 'tp'), may hold values from -6 to 6
- output_gate_logits: bfloat16 [16384, 1024], P('sp', 'tp'), may hold values from -6 to 6
- lower_bound_margin: float32 [1024], P('tp'), may hold values from 6.1035156e-05 to 0.08
- extra_forget_logs: float32 [16384, 1024], P('sp', 'tp'), may hold values from -0.7 to 0
- per_head_norm_gain: float32 [128], replicated, may hold values from 0.1 to 1.9
- output_weight: bfloat16 [1024, 2048], P('tp'), may hold values from -0.1875 to 0.1875
- feedforward_norm_gain: float32 [2048], replicated, may hold values from 0.1 to 1.9
- gate_weight: bfloat16 [2048, 5632], P('sp', 'tp'), may hold values from -0.125 to 0.125
- up_weight: bfloat16 [2048, 5632], P('sp', 'tp'), may hold values from -0.125 to 0.125
- down_weight: bfloat16 [5632, 2048], P('tp', 'sp'), may hold values from -0.078125 to 0.078125
Outputs:
- layer_out: bfloat16 [16384, 2048], P('sp')
All inputs are finite; a program needn't handle non-finite values.
Results may differ from a plain program's by a relative error of at most 0.015.
Values may be sent and summed in bfloat16 or wider, within the bound.
No kernel may reach another device: no remote copies, remote signals or barrier semaphores. Data moves between devices by JAX's collectives and lax.ppermute only.
A program may use at most 64 MiB of HBM per device.

v0:
```python
import jax
import jax.numpy as jnp
from jax import lax
from jax.experimental import pallas as pl
from jax.experimental.pallas import tpu as pltpu
from jax.sharding import Mesh
from jax.sharding import PartitionSpec as P


HD = 128
BLOCK = 64
SP = ("z", "y")
TP = ("x", "c")
SCALE = 2.0**18
STATE_SCALE = 2.0**10
NN = (((1,), (0,)), ((), ()))
NT = (((1,), (1,)), ((), ()))
TN = (((0,), (0,)), ((), ()))


eps = 1e-06


def shifted(value, axis, step):
    size = lax.axis_size(axis)
    return lax.ppermute(value, axis, [(k, (k + step) % size) for k in range(size)])


def whole(space=pltpu.VMEM):
    return pl.BlockSpec(memory_space=space)


def dot(left, right, dims=NN):
    return lax.dot_general(
        left.astype(jnp.bfloat16),
        right.astype(jnp.bfloat16),
        dims,
        preferred_element_type=jnp.float32,
    )


def halves(value):
    high = value.astype(jnp.bfloat16)
    return high, (value - high.astype(jnp.float32)).astype(jnp.bfloat16)


def scan_kernel(
    q_ref,
    f_ref,
    v_ref,
    margin_ref,
    extra_ref,
    gate_ref,
    up_ref,
    turned_ref,
    out_ref,
    scaled_ref,
    packed_ref,
):
    queries = q_ref[...].astype(jnp.float32)
    inflow = margin_ref[...] * jax.nn.sigmoid(-f_ref[...].astype(jnp.float32))
    keep_log = jnp.log1p(-inflow) + extra_ref[...]
    row = lax.broadcasted_iota(jnp.int32, (256, 256), 0)
    column = lax.broadcasted_iota(jnp.int32, (256, 256), 1)
    lower = (column <= row).astype(jnp.float32)
    total = jnp.dot(
        lower, keep_log, precision=lax.Precision.HIGHEST, preferred_element_type=jnp.float32
    )
    scaled_ref[...] = (queries * jnp.exp(total)).astype(jnp.bfloat16)
    causal = lax.broadcasted_iota(jnp.int32, (BLOCK, BLOCK), 1) <= lax.broadcasted_iota(
        jnp.int32, (BLOCK, BLOCK), 0
    )
    state = None
    ended = jnp.zeros((1, HD), jnp.float32)
    for k in range(256 // BLOCK):
        rows = slice(k * BLOCK, (k + 1) * BLOCK)
        inside, sums = queries[rows], total[rows]
        middle, end = sums[BLOCK // 2 - 1 : BLOCK // 2], sums[BLOCK - 1 :]
        values = v_ref[rows]
        scores = dot(inside * jnp.exp(sums - middle), inflow[rows] * jnp.exp(middle - sums), NT)
        result = dot(jnp.where(causal, scores, 0.0), values)
        added = dot(values, inflow[rows] * jnp.exp(end - sums), TN)
        if state is not None:
            result = result + dot(inside * jnp.exp(sums - ended), state, NT)
            added = added + jnp.exp(end - ended) * state
        out_ref[rows, :] = result
        state, ended = added, end
    packed = state.astype(jnp.bfloat16)
    for k in range(8):
        packed_ref[32:, k * 128 : (k + 1) * 128] = packed[k * 16 : (k + 1) * 16]
    high, low = halves(jnp.broadcast_to(ended, (16, HD)))
    packed_ref[32:, 1024:1152] = high
    packed_ref[32:, 1152:1280] = low
    packed_ref[32:, 1280:] = jnp.zeros((16, 256), jnp.bfloat16)
    for k in range(5):
        packed_ref[:32, k * 256 : k * 256 + 128] = gate_ref[:, k * 128 : (k + 1) * 128]
        packed_ref[:32, k * 256 + 128 : (k + 1) * 256] = up_ref[:, k * 128 : (k + 1) * 128]
    packed_ref[:32, 1280:1408] = jnp.concatenate([gate_ref[:, 640:], up_ref[:, 640:]], axis=1)
    packed_ref[:32, 1408:] = jnp.concatenate(
        [turned_ref[:, 640:], jnp.zeros((32, 64), jnp.bfloat16)], axis=1
    )


def scanned(*operands):
    return pl.pallas_call(
        scan_kernel,
        out_shape=(
            jax.ShapeDtypeStruct((256, HD), jnp.float32),
            jax.ShapeDtypeStruct((256, HD), jnp.bfloat16),
            jax.ShapeDtypeStruct((48, 1536), jnp.bfloat16),
        ),
        in_specs=[whole()] * 8,
        out_specs=(whole(),) * 3,
        cost_estimate=pl.CostEstimate(
            flops=4_000_000_000, bytes_accessed=500_000, transcendentals=300_000
        ),
        name="scan",
    )(*operands)


def y_kernel(y_ref, pieces_ref, turned_ref, total_ref, here_ref):
    y = y_ref[0]
    total_sum = here_sum = jnp.zeros((1, HD), jnp.float32)
    total = here = jnp.zeros((HD, HD), jnp.float32)
    for k in range(4):
        here = jnp.where(k == y, total, here)
        here_sum = jnp.where(k == y, total_sum, here_sum)
        state = jnp.concatenate(
            [pieces_ref[k, 32:, j * 128 : (j + 1) * 128] for j in range(8)], axis=0
        ).astype(jnp.float32)
        one = pieces_ref[k, 32:, 1024:1152].astype(jnp.float32)[:1]
        one = one + pieces_ref[k, 32:, 1152:1280].astype(jnp.float32)[:1]
        total = jnp.exp(one) * total + state
        total_sum = total_sum + one
    here_ref[:HD, :] = here
    here_ref[HD:, :] = jnp.broadcast_to(here_sum, (8, HD))
    total_ref[:32, :] = turned_ref[:, :640].astype(jnp.float32) * SCALE
    for k in range(4):
        total_ref[32:, k * 128 : (k + 1) * 128] = total[k * 32 : (k + 1) * 32] * STATE_SCALE
    total_ref[32:, 512:] = jnp.broadcast_to(total_sum, (32, HD))


def joined_over_y(y, pieces, turned):
    return pl.pallas_call(
        y_kernel,
        out_shape=(
            jax.ShapeDtypeStruct((64, 640), jnp.float32),
            jax.ShapeDtypeStruct((136, HD), jnp.float32),
        ),
        in_specs=[whole(pltpu.SMEM), whole(), whole()],
        out_specs=(whole(), whole()),
        cost_estimate=pl.CostEstimate(
            flops=1_000_000_000, bytes_accessed=700_000, transcendentals=1000
        ),
        name="join",
    )(y, pieces, turned)


def mix_kernel(z_ref, lines_ref, here_ref, out_ref, scaled_ref, logits_ref, gain_ref, gated_ref):
    z = z_ref[0]
    before = jnp.zeros((HD, HD), jnp.float32)
    for k in range(15):
        state = jnp.concatenate(
            [lines_ref[k, :, j * 128 : (j + 1) * 128] for j in range(4)], axis=0
        )
        joined = jnp.exp(lines_ref[k, :1, 512:]) * before + state
        before = jnp.where(k < z, joined, before)
    here = here_ref[...]
    state = jnp.exp(here[HD : HD + 1]) * (before * (1.0 / STATE_SCALE)) + here[:HD]
    mixed = out_ref[...] + dot(scaled_ref[...], state, NT)
    normed = mixed * lax.rsqrt(jnp.mean(mixed * mixed, axis=-1, keepdims=True) + eps)
    logits = logits_ref[...].astype(jnp.float32)
    gated = (normed * gain_ref[...] * (logits * jax.nn.sigmoid(logits))).astype(jnp.bfloat16)
    gated_ref[...] = gated


def mixed_rows(z, lines, here, out, scaled, logits, gain):
    return pl.pallas_call(
        mix_kernel,
        out_shape=jax.ShapeDtypeStruct((256, HD), jnp.bfloat16),
        in_specs=[whole(pltpu.SMEM)] + [whole()] * 6,
        out_specs=whole(),
        cost_estimate=pl.CostEstimate(
            flops=2_000_000_000, bytes_accessed=2_000_000, transcendentals=100_000
        ),
        name="mix",
    )(z, lines, here, out, scaled, logits, gain)


def ffn_kernel(
    core_ref,
    after_ref,
    gain_ref,
    wide_ref,
    pieces_ref,
    mine_ref,
    theirs_ref,
    bands,
    after_rows,
    pieces,
    normed,
    half,
    hidden,
    band_sems,
):
    core = core_ref[0]
    band_copies = [
        pltpu.make_async_copy(
            wide_ref.at[pl.ds(start, size)], bands.at[pl.ds(start, size)], band_sems.at[n]
        )
        for n, (start, size) in enumerate(((0, 512), (512, 1536)))
    ]
    after_copy = pltpu.make_async_copy(after_ref, after_rows, band_sems.at[2])
    piece_copy = pltpu.make_async_copy(pieces_ref, pieces, band_sems.at[3])
    after_copy.start()
    for copy in band_copies:
        copy.start()
    piece_copy.start()
    after_copy.wait()
    for k in range(8):
        lines = slice(k * 32, (k + 1) * 32)
        after = after_rows[lines].astype(jnp.float32)
        scale = lax.rsqrt(jnp.mean(after * after, axis=-1, keepdims=True) + eps)
        normed[lines] = (after * scale * gain_ref[...]).astype(jnp.bfloat16)
    spans = [slice(n * 256, min(n * 256 + 256, 1408)) for n in range(6)]
    rows = normed[:, :512]
    band_copies[0].wait()
    for span in spans:
        half[:, span] = jnp.dot(rows, bands[:512, span], preferred_element_type=jnp.float32)
    rows = normed[:, 512:]
    band_copies[1].wait()
    for n, span in enumerate(spans):
        both = half[:, span] + jnp.dot(
            rows, bands[512:, span], preferred_element_type=jnp.float32
        )
        width = both.shape[1] // 2
        gate, up = both[:, :width], both[:, width:]
        hidden[:, n * 128 : n * 128 + width] = (gate * jax.nn.sigmoid(gate) * up).astype(
            jnp.bfloat16
        )
    piece_copy.wait()
    first, second = hidden[:, :640], hidden[:, 640:704]

    @pl.loop(0, 8)
    def _(n):
        at = pl.multiple_of(n * 256, 256)
        part = lax.dot_general(
            first,
            jnp.concatenate(
                [pieces[k, n * 2 + j] for j in range(2) for k in range(4)], axis=0
            ),
            NT,
            preferred_element_type=jnp.float32,
        ) + lax.dot_general(
            second,
            bands[pl.ds(at, 256), 1408:1472],
            NT,
            preferred_element_type=jnp.float32,
        )
        part = part.astype(jnp.bfloat16).reshape(4, 2, 32, 256)
        mine_ref[:, :, pl.ds(at, 256)] = jnp.where(core == 0, part[:, 0], part[:, 1])
        theirs_ref[:, :, pl.ds(at, 256)] = jnp.where(core == 0, part[:, 1], part[:, 0])


def ffn(core, after, gain, wide, pieces):
    half = jax.ShapeDtypeStruct((4, 32, 2048), jnp.bfloat16)
    return pl.pallas_call(
        ffn_kernel,
        out_shape=(half, half),
        in_specs=[
            whole(pltpu.SMEM),
            whole(pltpu.HBM),
            whole(),
            whole(pltpu.HBM),
            whole(pltpu.HBM),
        ],
        out_specs=(whole(), whole()),
        scratch_shapes=[
            pltpu.VMEM((2048, 1536), jnp.bfloat16),
            pltpu.VMEM((256, 2048), jnp.bfloat16),
            pltpu.VMEM((4, 16, 32, 640), jnp.bfloat16),
            pltpu.VMEM((256, 2048), jnp.bfloat16),
            pltpu.VMEM((256, 1408), jnp.float32),
            pltpu.VMEM((256, 768), jnp.bfloat16),
            pltpu.SemaphoreType.DMA((4,)),
        ],
        compiler_params=pltpu.CompilerParams(vmem_limit_bytes=52 * 2**20),
        cost_estimate=pl.CostEstimate(
            flops=2 * 256 * 2048 * 2112, bytes_accessed=11 * 2**20, transcendentals=256 * 704
        ),
        name="ffn",
    )(core, after, gain, wide, pieces)


def local(
    residual,
    queries,
    forget_gate_logits,
    projected_values,
    output_gate_logits,
    lower_bound_margin,
    extra_forget_logs,
    per_head_norm_gain,
    output_weight,
    feedforward_norm_gain,
    gate_weight,
    up_weight,
    down_weight,
):
    y = lax.axis_index("y").reshape(1)
    z = lax.axis_index("z").reshape(1)
    core = lax.axis_index("c")
    turned = down_weight.T
    out_rows, scaled, packed = scanned(
        queries,
        forget_gate_logits,
        projected_values,
        lower_bound_margin.reshape(1, HD),
        extra_forget_logs,
        gate_weight,
        up_weight,
        turned,
    )
    along_y = lax.all_gather(packed, "y")
    wide = lax.all_gather(along_y[:, :32].reshape(128, 1536), "z", axis=0, tiled=True)
    out_copies = jnp.broadcast_to(output_weight, (4, *output_weight.shape))
    out_mine = lax.all_to_all(out_copies, "x", split_axis=0, concat_axis=0, tiled=True)
    total, here = joined_over_y(y, along_y, turned)
    along_z = lax.all_gather(total.astype(jnp.float16), "z")
    own = (along_z[:, :32].astype(jnp.float32) * (1.0 / SCALE)).astype(jnp.bfloat16)
    own = jnp.broadcast_to(own, (4, 16, 32, 640))
    pieces = lax.all_to_all(own, "y", split_axis=0, concat_axis=0, tiled=True)
    lines = along_z[:, 32:].astype(jnp.float32)
    lines, out_mine = lax.optimization_barrier((lines, out_mine))
    out_other = shifted(out_mine, "c", 1)
    gated = mixed_rows(
        z,
        lines,
        here,
        out_rows,
        scaled,
        output_gate_logits,
        per_head_norm_gain.reshape(1, HD),
    )
    heads = lax.all_gather(gated, "x")
    heads_other = shifted(heads, "c", 1)
    projected = 0.0
    for part, weight in ((heads, out_mine), (heads_other, out_other)):
        projected = projected + jnp.dot(
            part.transpose(1, 0, 2).reshape(256, 512),
            weight.reshape(512, 2048),
            preferred_element_type=jnp.float32,
        )
    after_mixer = (residual.astype(jnp.float32) + projected).astype(jnp.bfloat16)
    gain = feedforward_norm_gain.reshape(1, 2048)
    mine, theirs = ffn(core.reshape(1), after_mixer, gain, wide, pieces)
    swapped = shifted(theirs, "c", 1)
    pair = (mine.astype(jnp.float32) + swapped.astype(jnp.float32)).astype(jnp.bfloat16)
    place = lax.axis_index(TP) * 32
    own_rows = lax.dynamic_slice_in_dim(after_mixer, place, 32, 0)
    pair, own_rows = lax.optimization_barrier((pair, own_rows))
    arrived = lax.all_to_all(pair, "x", split_axis=0, concat_axis=0, tiled=True)
    ffn_sum = arrived.astype(jnp.float32).sum(axis=0)
    finished = (own_rows.astype(jnp.float32) + 0.5 * ffn_sum).astype(jnp.bfloat16)
    copies = jnp.broadcast_to(finished, (4, 32, 2048))
    along_x = lax.all_to_all(copies, "x", split_axis=0, concat_axis=0, tiled=True)
    others = shifted(along_x, "c", 1)
    first = jnp.where(core == 0, along_x, others)
    second = jnp.where(core == 0, others, along_x)
    return jnp.stack([first, second], axis=1).reshape(256, 2048)


def solution(mesh):
    finer = Mesh(mesh.devices.reshape(16, 4, 4, 2), ("z", "y", "x", "c"))
    placed = (
        P(SP, None),
        P(SP, TP),
        P(SP, TP),
        P(SP, TP),
        P(SP, TP),
        P(TP),
        P(SP, TP),
        P(),
        P(TP, None),
        P(),
        P(SP, TP),
        P(SP, TP),
        P(TP, SP),
    )
    return jax.shard_map(
        local, mesh=finer, in_specs=placed, out_specs=P(SP, None), check_vma=False
    )
```

profile of v0, /device:TPU:1, one launch (start us, length us, event | category | flops | bytes accessed | tf_op | source)
XLA Modules:
  0.0 185.4 jit_solution(17698932028349460688)
XLA Ops:
  6.5 3.0 %scan.1 = (f32[256,128]{1,0:T(8,128)}, bf16[256,128]{1,0:T(8,128)(2,1)}, bf16[48,1536]{1,0:T(8,128)(2,1)}) custom-call(bf16[256,128]{1,0:T(8,128)(2,1)} %q_ref.1, bf16[256,128]{1,0:T(8,128)(2,1)} %f_ref.1, bf16[256,128]{1,0:T(8,128)(2,1)} %v_ref.1, f32[1,128]{1,0:T(1,128)} %bitcast.46, f32[256,128]{1,0:T(8,128)} %extra_ref.1, bf16[32,704]{1,0:T(8,128)(2,1)} %gate_ref.1, ...), custom_call_target="tpu_custom_call" | custom-call | flops 4000000000 | bytes 500000 | tf_op jit(solution)/shard_map/scan/pallas_call | solution.py:105
  9.6 11.7 %all-gather = bf16[192,1536]{1,0:T(8,128)(2,1)S(1)} all-gather(bf16[48,1536]{1,0:T(8,128)(2,1)} %get-tuple-element.16), channel_id=2, replica_groups=mesh['z'=16,'y'=4,'x'=4,'c'=2] {'y'}, dimensions={0}, use_global_device_ids=true | all-gather | bytes 737280 | tf_op jit(solution)/shard_map/all_gather | solution.py:324
  22.1 1.6 broadcast_in_dim.9
  23.8 5.4 %all-to-all-start = ((bf16[4,128,2048]{2,1,0:T(8,128)(2,1)}), bf16[4,128,2048]{2,1,0:T(8,128)(2,1)}, u32[]{:S(2)}, u32[]{:S(2)}) async-start(bf16[4,128,2048]{2,1,0:T(8,128)(2,1)} %broadcast_in_dim.9), calls=%async_computation | async-start | bytes 4194304 | tf_op jit(solution)/shard_map/all_to_all | solution.py:327
  29.2 1.8 join.1
  31.9 53.6 %all-gather.7 = f16[1024,640]{1,0:T(8,128)(2,1)S(1)} all-gather(f16[64,640]{1,0:T(8,128)(2,1)S(1)} %convert_element_type.37), channel_id=3, replica_groups=mesh['z'=16,'y'=4,'x'=4,'c'=2] {'z'}, dimensions={0}, use_global_device_ids=true | all-gather | bytes 1392640 | tf_op jit(solution)/shard_map/all_gather | solution.py:329
  85.5 1.2 slice_convert_fusion.lines_ref
  86.7 9.9 %collective-permute-start.1 = (bf16[4,128,2048]{2,1,0:T(8,128)(2,1)}, bf16[4,128,2048]{2,1,0:T(8,128)(2,1)}, u32[]{:S(2)}, u32[]{:S(2)}) collective-permute-start(bf16[4,128,2048]{2,1,0:T(8,128)(2,1)} %all-to-all-done), channel_id=1, source_target_pairs={{0,1},{1,0},{2,3},{3,2},{4,5},{5,4},{6,7},{7,6},{8,9},{9,8},{10,11... | collective-permute-start | bytes 6291464 | tf_op jit(solution)/shard_map/ppermute | solution.py:26
  96.7 1.8 broadcast_in_dim.10
  98.5 3.7 %all-to-all-start.1 = ((bf16[4,16,32,640]{3,2,1,0:T(8,128)(2,1)}), bf16[4,16,32,640]{3,2,1,0:T(8,128)(2,1)S(1)}, u32[]{:S(2)}, u32[]{:S(2)}) async-start(bf16[4,16,32,640]{3,2,1,0:T(8,128)(2,1)} %broadcast_in_dim.10), calls=%async_computation.1 | async-start | bytes 5242880 | tf_op jit(solution)/shard_map/all_to_all | solution.py:332
  102.2 2.4 %mix.1 = bf16[256,128]{1,0:T(8,128)(2,1)} custom-call(s32[1]{0:T(128)} %bitcast.1.z_ref, f32[16,32,640]{2,1,0:T(8,128)} %slice_convert_fusion.lines_ref, f32[136,128]{1,0:T(8,128)} %get-tuple-element.19.here_ref, f32[256,128]{1,0:T(8,128)} %get-tuple-element.20.out_ref, bf16[256,128]{1,0:T(8,128)(2,1)} %get-tuple-element.21.scaled_ref, ...), custom_call_target="tpu_custom_call" | custom-call | flops 2000000000 | bytes 2000000 | tf_op jit(solution)/shard_map/mix/pallas_call | solution.py:178
  104.6 12.3 %all-gather.2 = bf16[1024,128]{1,0:T(8,128)(2,1)S(1)} all-gather(bf16[256,128]{1,0:T(8,128)(2,1)} %mix.1), channel_id=4, replica_groups=mesh['z'=16,'y'=4,'x'=4,'c'=2] {'x'}, dimensions={0}, use_global_device_ids=true | all-gather | bytes 327680 | tf_op jit(solution)/shard_map/all_gather | solution.py:345
  116.8 3.9 %collective-permute-start = (bf16[4,256,128]{2,1,0:T(8,128)(2,1)S(1)}, bf16[4,256,128]{2,1,0:T(8,128)(2,1)S(1)}, u32[]{:S(2)}, u32[]{:S(2)}) collective-permute-start(bf16[4,256,128]{2,1,0:T(8,128)(2,1)S(1)} %bitcast.42), channel_id=1, source_target_pairs={{0,1},{1,0},{2,3},{3,2},{4,5},{5,4},{6,7},{7,6},{8,9},{9,8},{10,11... | collective-permute-start | bytes 786440 | tf_op jit(solution)/shard_map/ppermute | solution.py:26
  120.7 2.4 %convolution_bitcast_fusion.1 = f32[256,2048]{1,0:T(8,128)S(1)} fusion(bf16[256,4,128]{2,0,1:T(8,128)(2,1)S(1)} %bitcast.43, bf16[4,128,2048]{2,1,0:T(8,128)(2,1)} %all-to-all-done), kind=kOutput, calls=%fused_computation.1 | convolution fusion | flops 536870912 | bytes 4456448 | tf_op jit(solution)/shard_map/dot_general | solution.py:349
  123.2 3.3 %fusion.2.after_ref = bf16[256,2048]{1,0:T(8,128)(2,1)} fusion(f32[256,2048]{1,0:T(8,128)S(1)} %convolution_bitcast_fusion.1, bf16[4,128,2048]{2,1,0:T(8,128)(2,1)} %collective-permute-done.1, bf16[256,2048]{1,0:T(8,128)(2,1)S(1)} %copy-done.3, bf16[4,256,128]{2,1,0:T(8,128)(2,1)S(1)} %collective-permute-done), kind=kOutput, calls=%fused_computation.4 | convolution fusion | flops 538968064 | bytes 6553600 | tf_op jit(solution)/shard_map/dot_general | solution.py:349
  126.5 7.6 %all-to-all-done.1.pieces_ref = bf16[4,16,32,640]{3,2,1,0:T(8,128)(2,1)S(1)} async-done(((bf16[4,16,32,640]{3,2,1,0:T(8,128)(2,1)}), bf16[4,16,32,640]{3,2,1,0:T(8,128)(2,1)S(1)}, u32[]{:S(2)}, u32[]{:S(2)}) %all-to-all-start.1) | async-done | bytes 2621472 | tf_op jit(solution)/shard_map/all_to_all | solution.py:332
  134.1 1.5 copy-done.1
  135.7 7.2 %ffn.1 = (bf16[4,32,2048]{2,1,0:T(8,128)(2,1)S(1)}, bf16[4,32,2048]{2,1,0:T(8,128)(2,1)S(1)}) custom-call(s32[1]{0:T(128)} %bitcast.core_ref, bf16[256,2048]{1,0:T(8,128)(2,1)} %fusion.2.after_ref, f32[1,2048]{1,0:T(1,128)S(1)} %bitcast.36, bf16[2048,1536]{1,0:T(8,128)(2,1)} %all-gather.6.cloned.1.call-done.wide_ref, bf16[4,16,32,640]{3,2,1,0:T(8,128)(2,1)} %copy-done.1), custom_call_target="tpu_custom_call" | custom-call | flops 2214592512 | bytes 11534336 | tf_op jit(solution)/shard_map/ffn/pallas_call | solution.py:267
  142.9 2.8 %collective-permute-start.2 = (bf16[4,32,2048]{2,1,0:T(8,128)(2,1)S(1)}, bf16[4,32,2048]{2,1,0:T(8,128)(2,1)S(1)}, u32[]{:S(2)}, u32[]{:S(2)}) collective-permute-start(bf16[4,32,2048]{2,1,0:T(8,128)(2,1)S(1)} %get-tuple-element.24), channel_id=1, source_target_pairs={{0,1},{1,0},{2,3},{3,2},{4,5},{5,4},{6,7},{7,6},{8,9},{9,8},{10,11... | collective-permute-start | bytes 1572872 | tf_op jit(solution)/shard_map/ppermute | solution.py:26
  147.4 13.6 %all_to_all.20 = bf16[4,32,2048]{2,1,0:T(8,128)(2,1)S(1)} all-to-all(bf16[4,32,2048]{2,1,0:T(8,128)(2,1)S(1)} %add_convert_fusion), channel_id=1, replica_groups=mesh['z'=16,'y'=4,'x'=4,'c'=2] {'x'}, dimensions={0} | all-to-all | bytes 1048576 | tf_op jit(solution)/shard_map/all_to_all | solution.py:362
  161.1 10.2 %all_to_all.21 = bf16[4,32,2048]{2,1,0:T(8,128)(2,1)S(1)} all-to-all(bf16[4,32,2048]{2,1,0:T(8,128)(2,1)S(1)} %broadcast_in_dim.11), channel_id=1, replica_groups=mesh['z'=16,'y'=4,'x'=4,'c'=2] {'x'}, dimensions={0} | all-to-all | bytes 1048576 | tf_op jit(solution)/shard_map/all_to_all | solution.py:366
  171.3 4.6 %collective-permute-start.3 = (bf16[4,32,2048]{2,1,0:T(8,128)(2,1)S(1)}, bf16[4,32,2048]{2,1,0:T(8,128)(2,1)S(1)}, u32[]{:S(2)}, u32[]{:S(2)}) collective-permute-start(bf16[4,32,2048]{2,1,0:T(8,128)(2,1)S(1)} %all_to_all.21), channel_id=1, source_target_pairs={{0,1},{1,0},{2,3},{3,2},{4,5},{5,4},{6,7},{7,6},{8,9},{9,8},{10,11... | collective-permute-start | bytes 1572872 | tf_op jit(solution)/shard_map/ppermute | solution.py:26
  175.9 1.5 collective-permute-done.3
  177.5 1.1 pad_maximum_fusion
  (25 shorter events, 3.8 us)
Async XLA Ops:
  6.5 127.6 %all-gather.6.cloned.1.call-start = ((), (), s32[]{:S(2)}) async-start(), calls=%async_computation.4 | async-start | bytes 6684672 | tf_op jit(solution)/shard_map/all_gather | solution.py:325
  9.6 12.6 %copy-start.4 = (bf16[128,2048]{1,0:T(8,128)(2,1)S(1)}, bf16[128,2048]{1,0:T(8,128)(2,1)}, u32[]{:S(2)}) copy-start(bf16[128,2048]{1,0:T(8,128)(2,1)} %param.21) | copy-start | bytes 1572868
  21.3 2.5 %copy-start.2 = (bf16[192,1536]{1,0:T(8,128)(2,1)}, bf16[192,1536]{1,0:T(8,128)(2,1)S(1)}, u32[]{:S(2)}) copy-start(bf16[192,1536]{1,0:T(8,128)(2,1)S(1)} %all-gather) | copy-start | bytes 1769476
  23.8 62.9 %all-to-all-start = ((bf16[4,128,2048]{2,1,0:T(8,128)(2,1)}), bf16[4,128,2048]{2,1,0:T(8,128)(2,1)}, u32[]{:S(2)}, u32[]{:S(2)}) async-start(bf16[4,128,2048]{2,1,0:T(8,128)(2,1)} %broadcast_in_dim.9), calls=%async_computation | async-start | bytes 4194304 | tf_op jit(solution)/shard_map/all_to_all | solution.py:327
  86.7 36.5 %collective-permute-start.1 = (bf16[4,128,2048]{2,1,0:T(8,128)(2,1)}, bf16[4,128,2048]{2,1,0:T(8,128)(2,1)}, u32[]{:S(2)}, u32[]{:S(2)}) collective-permute-start(bf16[4,128,2048]{2,1,0:T(8,128)(2,1)} %all-to-all-done), channel_id=1, source_target_pairs={{0,1},{1,0},{2,3},{3,2},{4,5},{5,4},{6,7},{7,6},{8,9},{9,8},{10,11... | collective-permute-start | bytes 6291464 | tf_op jit(solution)/shard_map/ppermute | solution.py:26
  98.5 35.6 %all-to-all-start.1 = ((bf16[4,16,32,640]{3,2,1,0:T(8,128)(2,1)}), bf16[4,16,32,640]{3,2,1,0:T(8,128)(2,1)S(1)}, u32[]{:S(2)}, u32[]{:S(2)}) async-start(bf16[4,16,32,640]{3,2,1,0:T(8,128)(2,1)} %broadcast_in_dim.10), calls=%async_computation.1 | async-start | bytes 5242880 | tf_op jit(solution)/shard_map/all_to_all | solution.py:332
  116.8 6.3 %collective-permute-start = (bf16[4,256,128]{2,1,0:T(8,128)(2,1)S(1)}, bf16[4,256,128]{2,1,0:T(8,128)(2,1)S(1)}, u32[]{:S(2)}, u32[]{:S(2)}) collective-permute-start(bf16[4,256,128]{2,1,0:T(8,128)(2,1)S(1)} %bitcast.42), channel_id=1, source_target_pairs={{0,1},{1,0},{2,3},{3,2},{4,5},{5,4},{6,7},{7,6},{8,9},{9,8},{10,11... | collective-permute-start | bytes 786440 | tf_op jit(solution)/shard_map/ppermute | solution.py:26
  120.7 2.4 %copy-start.3 = (bf16[256,2048]{1,0:T(8,128)(2,1)S(1)}, bf16[256,2048]{1,0:T(8,128)(2,1)}, u32[]{:S(2)}) copy-start(bf16[256,2048]{1,0:T(8,128)(2,1)} %param.13) | copy-start | bytes 3145732
  123.1 12.6 %copy-start = (f32[2048]{0:T(1024)S(1)}, f32[2048]{0:T(1024)}, u32[]{:S(2)}) copy-start(f32[2048]{0:T(1024)} %param.22) | copy-start | bytes 24580
  134.1 1.6 copy-start.1
  142.9 4.3 %collective-permute-start.2 = (bf16[4,32,2048]{2,1,0:T(8,128)(2,1)S(1)}, bf16[4,32,2048]{2,1,0:T(8,128)(2,1)S(1)}, u32[]{:S(2)}, u32[]{:S(2)}) collective-permute-start(bf16[4,32,2048]{2,1,0:T(8,128)(2,1)S(1)} %get-tuple-element.24), channel_id=1, source_target_pairs={{0,1},{1,0},{2,3},{3,2},{4,5},{5,4},{6,7},{7,6},{8,9},{9,8},{10,11... | collective-permute-start | bytes 1572872 | tf_op jit(solution)/shard_map/ppermute | solution.py:26
  171.3 6.1 %collective-permute-start.3 = (bf16[4,32,2048]{2,1,0:T(8,128)(2,1)S(1)}, bf16[4,32,2048]{2,1,0:T(8,128)(2,1)S(1)}, u32[]{:S(2)}, u32[]{:S(2)}) collective-permute-start(bf16[4,32,2048]{2,1,0:T(8,128)(2,1)S(1)} %all_to_all.21), channel_id=1, source_target_pairs={{0,1},{1,0},{2,3},{3,2},{4,5},{5,4},{6,7},{7,6},{8,9},{9,8},{10,11... | collective-permute-start | bytes 1572872 | tf_op jit(solution)/shard_map/ppermute | solution.py:26
Sparse Core Ops, SparseCore 0:
  22.2 102.8 all-gather.5
where the time goes:
time: 186 us; the launch traced here: 185 us
  blocking collectives  101 us (54%)
  starting transfers between devices  30.1 us (16%)
  Pallas kernels  14.5 us (8%)
  between operations  13.6 us (7%)
  waiting for transfers between devices  9.74 us (5%)
  local copies, waits for them, and re-layouts  6.8 us (4%)
  matrix products  5.73 us (3%)
  other arithmetic  3.59 us (2%)
    all_gather x1, blocking collectives, local(): along_z = lax.all_gather(total.astype(jnp.float16), 'z')  53.6 us
    ppermute x4, starting transfers between devices, shifted(): lax.ppermute(value, axis, [(k, (k + step) % size) for k in range(size)])  21.1 us
    all_to_all x1, blocking collectives, local(): arrived = lax.all_to_all(pair, 'x', split_axis=0, concat_axis=0, tiled=True)  13.6 us
    all_gather x1, blocking collectives, local(): heads = lax.all_gather(gated, 'x')  12.3 us
    all_gather x1, blocking collectives, local(): along_y = lax.all_gather(packed, 'y')  11.7 us
    all_to_all x1, blocking collectives, local(): lax.all_to_all(copies, 'x', split_axis=0, concat_axis=0, tiled=True)  10.2 us
    all_to_all x1, waiting for transfers between devices, local(): pieces = lax.all_to_all(own, 'y', split_axis=0, concat_axis=0, tiled=True)  7.62 us
    pallas_call x1, Pallas kernels, ffn(): pl.pallas_call(ffn_kernel, out_shape=(half, half), in_specs=[whole(pltpu....  7.2 us
  transfers between devices with their start and end apart: 7, of which 3 were waited for; matrix products, arithmetic and copies ran while one was open for 7% of the time, Pallas kernels for 2%

commit v1 on v0

--- a/solution.py
+++ b/solution.py
@@ -52,7 +52,6 @@
     extra_ref,
     gate_ref,
     up_ref,
-    turned_ref,
     out_ref,
     scaled_ref,
     packed_ref,
@@ -91,14 +90,11 @@
     high, low = halves(jnp.broadcast_to(ended, (16, HD)))
     packed_ref[32:, 1024:1152] = high
     packed_ref[32:, 1152:1280] = low
-    packed_ref[32:, 1280:] = jnp.zeros((16, 256), jnp.bfloat16)
+    packed_ref[32:, 1280:] = jnp.zeros((16, 128), jnp.bfloat16)
     for k in range(5):
         packed_ref[:32, k * 256 : k * 256 + 128] = gate_ref[:, k * 128 : (k + 1) * 128]
         packed_ref[:32, k * 256 + 128 : (k + 1) * 256] = up_ref[:, k * 128 : (k + 1) * 128]
     packed_ref[:32, 1280:1408] = jnp.concatenate([gate_ref[:, 640:], up_ref[:, 640:]], axis=1)
-    packed_ref[:32, 1408:] = jnp.concatenate(
-        [turned_ref[:, 640:], jnp.zeros((32, 64), jnp.bfloat16)], axis=1
-    )
 
 
 def scanned(*operands):
@@ -107,9 +103,9 @@
         out_shape=(
             jax.ShapeDtypeStruct((256, HD), jnp.float32),
             jax.ShapeDtypeStruct((256, HD), jnp.bfloat16),
-            jax.ShapeDtypeStruct((48, 1536), jnp.bfloat16),
-        ),
-        in_specs=[whole()] * 8,
+            jax.ShapeDtypeStruct((48, 1408), jnp.bfloat16),
+        ),
+        in_specs=[whole()] * 7,
         out_specs=(whole(),) * 3,
         cost_estimate=pl.CostEstimate(
             flops=4_000_000_000, bytes_accessed=500_000, transcendentals=300_000
@@ -134,17 +130,19 @@
         total_sum = total_sum + one
     here_ref[:HD, :] = here
     here_ref[HD:, :] = jnp.broadcast_to(here_sum, (8, HD))
-    total_ref[:32, :] = turned_ref[:, :640].astype(jnp.float32) * SCALE
+    total_ref[:32, :704] = turned_ref[...].astype(jnp.float32) * SCALE
+    total_ref[:32, 704:] = jnp.zeros((32, 64), jnp.float32)
     for k in range(4):
         total_ref[32:, k * 128 : (k + 1) * 128] = total[k * 32 : (k + 1) * 32] * STATE_SCALE
-    total_ref[32:, 512:] = jnp.broadcast_to(total_sum, (32, HD))
+    total_ref[32:, 512:640] = jnp.broadcast_to(total_sum, (32, HD))
+    total_ref[32:, 640:] = jnp.zeros((32, HD), jnp.float32)
 
 
 def joined_over_y(y, pieces, turned):
     return pl.pallas_call(
         y_kernel,
         out_shape=(
-            jax.ShapeDtypeStruct((64, 640), jnp.float32),
+            jax.ShapeDtypeStruct((64, 768), jnp.float32),
             jax.ShapeDtypeStruct((136, HD), jnp.float32),
         ),
         in_specs=[whole(pltpu.SMEM), whole(), whole()],
@@ -163,7 +161,7 @@
         state = jnp.concatenate(
             [lines_ref[k, :, j * 128 : (j + 1) * 128] for j in range(4)], axis=0
         )
-        joined = jnp.exp(lines_ref[k, :1, 512:]) * before + state
+        joined = jnp.exp(lines_ref[k, :1, 512:640]) * before + state
         before = jnp.where(k < z, joined, before)
     here = here_ref[...]
     state = jnp.exp(here[HD : HD + 1]) * (before * (1.0 / STATE_SCALE)) + here[:HD]
@@ -239,21 +237,16 @@
             jnp.bfloat16
         )
     piece_copy.wait()
-    first, second = hidden[:, :640], hidden[:, 640:704]
+    inner = hidden[:, :704]
 
     @pl.loop(0, 8)
     def _(n):
         at = pl.multiple_of(n * 256, 256)
         part = lax.dot_general(
-            first,
+            inner,
             jnp.concatenate(
-                [pieces[k, n * 2 + j] for j in range(2) for k in range(4)], axis=0
+                [pieces[k, n * 2 + j, :, :704] for j in range(2) for k in range(4)], axis=0
             ),
-            NT,
-            preferred_element_type=jnp.float32,
-        ) + lax.dot_general(
-            second,
-            bands[pl.ds(at, 256), 1408:1472],
             NT,
             preferred_element_type=jnp.float32,
         )
@@ -276,9 +269,9 @@
         ],
         out_specs=(whole(), whole()),
         scratch_shapes=[
-            pltpu.VMEM((2048, 1536), jnp.bfloat16),
+            pltpu.VMEM((2048, 1408), jnp.bfloat16),
             pltpu.VMEM((256, 2048), jnp.bfloat16),
-            pltpu.VMEM((4, 16, 32, 640), jnp.bfloat16),
+            pltpu.VMEM((4, 16, 32, 768), jnp.bfloat16),
             pltpu.VMEM((256, 2048), jnp.bfloat16),
             pltpu.VMEM((256, 1408), jnp.float32),
             pltpu.VMEM((256, 768), jnp.bfloat16),
@@ -319,16 +312,15 @@
         extra_forget_logs,
         gate_weight,
         up_weight,
-        turned,
     )
     along_y = lax.all_gather(packed, "y")
-    wide = lax.all_gather(along_y[:, :32].reshape(128, 1536), "z", axis=0, tiled=True)
+    wide = lax.all_gather(along_y[:, :32].reshape(128, 1408), "z", axis=0, tiled=True)
     out_copies = jnp.broadcast_to(output_weight, (4, *output_weight.shape))
     out_mine = lax.all_to_all(out_copies, "x", split_axis=0, concat_axis=0, tiled=True)
     total, here = joined_over_y(y, along_y, turned)
     along_z = lax.all_gather(total.astype(jnp.float16), "z")
     own = (along_z[:, :32].astype(jnp.float32) * (1.0 / SCALE)).astype(jnp.bfloat16)
-    own = jnp.broadcast_to(own, (4, 16, 32, 640))
+    own = jnp.broadcast_to(own, (4, 16, 32, 768))
     pieces = lax.all_to_all(own, "y", split_axis=0, concat_axis=0, tiled=True)
     lines = along_z[:, 32:].astype(jnp.float32)
     lines, out_mine = lax.optimization_barrier((lines, out_mine))

time: 186 us -> 195 us (1.048)
  waiting for transfers between devices: 9.74 us -> 18.7 us
    all_to_all x1, waiting for transfers between devices: 7.62 us -> 16.2 us  [local(): pieces = lax.all_to_all(own, 'y', split_axis=0, concat_axis=0, tiled=True)]
    all_gather x1, blocking collectives: 53.6 us -> 57.5 us  [local(): along_z = lax.all_gather(total.astype(jnp.float16), 'z')]
    all_to_all x1, blocking collectives: 13.6 us -> 11.2 us  [local(): arrived = lax.all_to_all(pair, 'x', split_axis=0, concat_axis=0, tiled=True)]
  transfers between devices with their start and end apart: 7 -> 7, of which waited for: 3 -> 4; matrix products, arithmetic and copies ran while one was open for 7% -> 6% of each run, Pallas kernels for 2% -> 2%
where the time goes in v1:
time: 195 us
  blocking collectives  101 us (52%)
  starting transfers between devices  31 us (16%)
  waiting for transfers between devices  18.7 us (10%)
  Pallas kernels  14.4 us (7%)
  between operations  13.5 us (7%)
  local copies, waits for them, and re-layouts  6.72 us (3%)
  other arithmetic  4.9 us (3%)
  matrix products  4.04 us (2%)
    all_gather x1, blocking collectives, local(): along_z = lax.all_gather(total.astype(jnp.float16), 'z')  57.5 us
    ppermute x4, starting transfers between devices, shifted(): lax.ppermute(value, axis, [(k, (k + step) % size) for k in range(size)])  20.9 us
    all_to_all x1, waiting for transfers between devices, local(): pieces = lax.all_to_all(own, 'y', split_axis=0, concat_axis=0, tiled=True)  16.2 us
    all_gather x1, blocking collectives, local(): along_y = lax.all_gather(packed, 'y')  11.6 us
    all_to_all x1, blocking collectives, local(): arrived = lax.all_to_all(pair, 'x', split_axis=0, concat_axis=0, tiled=True)  11.2 us
    all_gather x1, blocking collectives, local(): heads = lax.all_gather(gated, 'x')  10.8 us
    all_to_all x1, blocking collectives, local(): lax.all_to_all(copies, 'x', split_axis=0, concat_axis=0, tiled=True)  10.2 us
    pallas_call x1, Pallas kernels, ffn(): pl.pallas_call(ffn_kernel, out_shape=(half, half), in_specs=[whole(pltpu....  7.08 us
  transfers between devices with their start and end apart: 7, of which 4 were waited for; matrix products, arithmetic and copies ran while one was open for 6% of the time, Pallas kernels for 2%

profile of v1, /device:TPU:1, one launch (start us, length us, event | category | flops | bytes accessed | tf_op | source)
XLA Modules:
  0.0 194.6 jit_solution(9827198837933162090)
XLA Ops:
  6.5 3.0 %scan.1 = (f32[256,128]{1,0:T(8,128)}, bf16[256,128]{1,0:T(8,128)(2,1)}, bf16[48,1408]{1,0:T(8,128)(2,1)}) custom-call(bf16[256,128]{1,0:T(8,128)(2,1)} %q_ref.1, bf16[256,128]{1,0:T(8,128)(2,1)} %f_ref.1, bf16[256,128]{1,0:T(8,128)(2,1)} %v_ref.1, f32[1,128]{1,0:T(1,128)} %bitcast.45, f32[256,128]{1,0:T(8,128)} %extra_ref.1, bf16[32,704]{1,0:T(8,128)(2,1)} %gate_ref.1, ...), custom_call_target="tpu_custom_call" | custom-call | flops 4000000000 | bytes 500000 | tf_op jit(solution)/shard_map/scan/pallas_call | solution.py:101
  9.6 11.6 %all-gather = bf16[192,1408]{1,0:T(8,128)(2,1)S(1)} all-gather(bf16[48,1408]{1,0:T(8,128)(2,1)} %get-tuple-element.16), channel_id=2, replica_groups=mesh['z'=16,'y'=4,'x'=4,'c'=2] {'y'}, dimensions={0}, use_global_device_ids=true | all-gather | bytes 675840 | tf_op jit(solution)/shard_map/all_gather | solution.py:316
  22.0 1.6 broadcast_in_dim.9
  23.6 5.4 %all-to-all-start = ((bf16[4,128,2048]{2,1,0:T(8,128)(2,1)}), bf16[4,128,2048]{2,1,0:T(8,128)(2,1)S(1)}, u32[]{:S(2)}, u32[]{:S(2)}) async-start(bf16[4,128,2048]{2,1,0:T(8,128)(2,1)} %broadcast_in_dim.9), calls=%async_computation | async-start | bytes 4194304 | tf_op jit(solution)/shard_map/all_to_all | solution.py:319
  29.0 1.8 join.1
  31.7 57.5 %all-gather.7 = f16[1024,768]{1,0:T(8,128)(2,1)S(1)} all-gather(f16[64,768]{1,0:T(8,128)(2,1)S(1)} %convert_element_type.37), channel_id=3, replica_groups=mesh['z'=16,'y'=4,'x'=4,'c'=2] {'z'}, dimensions={0}, use_global_device_ids=true | all-gather | bytes 1671168 | tf_op jit(solution)/shard_map/all_gather | solution.py:321
  89.2 1.2 copy-done.1
  90.5 1.3 slice_convert_fusion.lines_ref
  91.8 10.0 %collective-permute-start.1 = (bf16[4,128,2048]{2,1,0:T(8,128)(2,1)S(1)}, bf16[4,128,2048]{2,1,0:T(8,128)(2,1)}, u32[]{:S(2)}, u32[]{:S(2)}) collective-permute-start(bf16[4,128,2048]{2,1,0:T(8,128)(2,1)S(1)} %all-to-all-done), channel_id=1, source_target_pairs={{0,1},{1,0},{2,3},{3,2},{4,5},{5,4},{6,7},{7,6},{8,9},{9,8},{10,11... | collective-permute-start | bytes 6291464 | tf_op jit(solution)/shard_map/ppermute | solution.py:26
  101.7 1.3 multiply_convert_fusion
  103.0 2.0 %broadcast_in_dim.10 = bf16[4,16,32,768]{3,2,1,0:T(8,128)(2,1)} broadcast(bf16[16,32,768]{2,1,0:T(8,128)(2,1)S(1)} %multiply_convert_fusion), dimensions={1,2,3} | broadcast | bytes 3932160 | tf_op jit(solution)/shard_map/broadcast_in_dim | solution.py:323
  105.0 4.7 %all-to-all-start.1 = ((bf16[4,16,32,768]{3,2,1,0:T(8,128)(2,1)}), bf16[4,16,32,768]{3,2,1,0:T(8,128)(2,1)}, u32[]{:S(2)}, u32[]{:S(2)}) async-start(bf16[4,16,32,768]{3,2,1,0:T(8,128)(2,1)} %broadcast_in_dim.10), calls=%async_computation.1 | async-start | bytes 6291456 | tf_op jit(solution)/shard_map/all_to_all | solution.py:324
  109.7 2.5 %mix.1 = bf16[256,128]{1,0:T(8,128)(2,1)} custom-call(s32[1]{0:T(128)} %bitcast.1.z_ref, f32[16,32,768]{2,1,0:T(8,128)} %slice_convert_fusion.lines_ref, f32[136,128]{1,0:T(8,128)} %get-tuple-element.19.here_ref, f32[256,128]{1,0:T(8,128)} %get-tuple-element.20.out_ref, bf16[256,128]{1,0:T(8,128)(2,1)} %get-tuple-element.21.scaled_ref, ...), custom_call_target="tpu_custom_call" | custom-call | flops 2000000000 | bytes 2000000 | tf_op jit(solution)/shard_map/mix/pallas_call | solution.py:176
  112.3 10.8 %all-gather.2 = bf16[1024,128]{1,0:T(8,128)(2,1)S(1)} all-gather(bf16[256,128]{1,0:T(8,128)(2,1)} %mix.1), channel_id=4, replica_groups=mesh['z'=16,'y'=4,'x'=4,'c'=2] {'x'}, dimensions={0}, use_global_device_ids=true | all-gather | bytes 327680 | tf_op jit(solution)/shard_map/all_gather | solution.py:337
  123.0 3.6 %collective-permute-start = (bf16[4,256,128]{2,1,0:T(8,128)(2,1)S(1)}, bf16[4,256,128]{2,1,0:T(8,128)(2,1)S(1)}, u32[]{:S(2)}, u32[]{:S(2)}) collective-permute-start(bf16[4,256,128]{2,1,0:T(8,128)(2,1)S(1)} %bitcast.42), channel_id=1, source_target_pairs={{0,1},{1,0},{2,3},{3,2},{4,5},{5,4},{6,7},{7,6},{8,9},{9,8},{10,11... | collective-permute-start | bytes 786440 | tf_op jit(solution)/shard_map/ppermute | solution.py:26
  127.9 3.3 %fusion.2.after_ref = bf16[256,2048]{1,0:T(8,128)(2,1)} fusion(f32[256,2048]{1,0:T(8,128)S(1)} %convolution_bitcast_fusion.1, bf16[4,128,2048]{2,1,0:T(8,128)(2,1)} %collective-permute-done.1, bf16[256,2048]{1,0:T(8,128)(2,1)S(1)} %copy-done.3, bf16[4,256,128]{2,1,0:T(8,128)(2,1)S(1)} %collective-permute-done), kind=kOutput, calls=%fused_computation.4 | convolution fusion | flops 538968064 | bytes 6553600 | tf_op jit(solution)/shard_map/dot_general | solution.py:341
  131.2 16.2 %all-to-all-done.1.pieces_ref = bf16[4,16,32,768]{3,2,1,0:T(8,128)(2,1)} async-done(((bf16[4,16,32,768]{3,2,1,0:T(8,128)(2,1)}), bf16[4,16,32,768]{3,2,1,0:T(8,128)(2,1)}, u32[]{:S(2)}, u32[]{:S(2)}) %all-to-all-start.1) | async-done | bytes 3145760 | tf_op jit(solution)/shard_map/all_to_all | solution.py:324
  147.5 7.1 %ffn.1 = (bf16[4,32,2048]{2,1,0:T(8,128)(2,1)S(1)}, bf16[4,32,2048]{2,1,0:T(8,128)(2,1)S(1)}) custom-call(s32[1]{0:T(128)} %bitcast.core_ref, bf16[256,2048]{1,0:T(8,128)(2,1)} %fusion.2.after_ref, f32[1,2048]{1,0:T(1,128)S(1)} %bitcast.36, bf16[2048,1408]{1,0:T(8,128)(2,1)} %all-gather.6.cloned.1.call-done.wide_ref, ...), custom_call_target="tpu_custom_call" | custom-call | flops 2214592512 | bytes 11534336 | tf_op jit(solution)/shard_map/ffn/pallas_call | solution.py:260
  154.5 2.8 %collective-permute-start.2 = (bf16[4,32,2048]{2,1,0:T(8,128)(2,1)S(1)}, bf16[4,32,2048]{2,1,0:T(8,128)(2,1)S(1)}, u32[]{:S(2)}, u32[]{:S(2)}) collective-permute-start(bf16[4,32,2048]{2,1,0:T(8,128)(2,1)S(1)} %get-tuple-element.24), channel_id=1, source_target_pairs={{0,1},{1,0},{2,3},{3,2},{4,5},{5,4},{6,7},{7,6},{8,9},{9,8},{10,11... | collective-permute-start | bytes 1572872 | tf_op jit(solution)/shard_map/ppermute | solution.py:26
  159.0 11.2 %all_to_all.20 = bf16[4,32,2048]{2,1,0:T(8,128)(2,1)S(1)} all-to-all(bf16[4,32,2048]{2,1,0:T(8,128)(2,1)S(1)} %add_convert_fusion), channel_id=1, replica_groups=mesh['z'=16,'y'=4,'x'=4,'c'=2] {'x'}, dimensions={0} | all-to-all | bytes 1048576 | tf_op jit(solution)/shard_map/all_to_all | solution.py:354
  170.4 10.2 %all_to_all.21 = bf16[4,32,2048]{2,1,0:T(8,128)(2,1)S(1)} all-to-all(bf16[4,32,2048]{2,1,0:T(8,128)(2,1)S(1)} %broadcast_in_dim.11), channel_id=1, replica_groups=mesh['z'=16,'y'=4,'x'=4,'c'=2] {'x'}, dimensions={0} | all-to-all | bytes 1048576 | tf_op jit(solution)/shard_map/all_to_all | solution.py:358
  180.5 4.6 %collective-permute-start.3 = (bf16[4,32,2048]{2,1,0:T(8,128)(2,1)S(1)}, bf16[4,32,2048]{2,1,0:T(8,128)(2,1)S(1)}, u32[]{:S(2)}, u32[]{:S(2)}) collective-permute-start(bf16[4,32,2048]{2,1,0:T(8,128)(2,1)S(1)} %all_to_all.21), channel_id=1, source_target_pairs={{0,1},{1,0},{2,3},{3,2},{4,5},{5,4},{6,7},{7,6},{8,9},{9,8},{10,11... | collective-permute-start | bytes 1572872 | tf_op jit(solution)/shard_map/ppermute | solution.py:26
  185.1 1.5 collective-permute-done.3
  186.7 1.1 pad_maximum_fusion
  (25 shorter events, 4.9 us)
Async XLA Ops:
  6.5 140.9 %all-gather.6.cloned.1.call-start = ((), (), s32[]{:S(2)}) async-start(), calls=%async_computation.4 | async-start | bytes 6127616 | tf_op jit(solution)/shard_map/all_gather | solution.py:317
  9.6 12.5 %copy-start.4 = (bf16[128,2048]{1,0:T(8,128)(2,1)S(1)}, bf16[128,2048]{1,0:T(8,128)(2,1)}, u32[]{:S(2)}) copy-start(bf16[128,2048]{1,0:T(8,128)(2,1)} %param.21) | copy-start | bytes 1572868
  21.2 2.4 %copy-start.2 = (bf16[192,1408]{1,0:T(8,128)(2,1)}, bf16[192,1408]{1,0:T(8,128)(2,1)S(1)}, u32[]{:S(2)}) copy-start(bf16[192,1408]{1,0:T(8,128)(2,1)S(1)} %all-gather) | copy-start | bytes 1622020
  23.6 68.2 %all-to-all-start = ((bf16[4,128,2048]{2,1,0:T(8,128)(2,1)}), bf16[4,128,2048]{2,1,0:T(8,128)(2,1)S(1)}, u32[]{:S(2)}, u32[]{:S(2)}) async-start(bf16[4,128,2048]{2,1,0:T(8,128)(2,1)} %broadcast_in_dim.9), calls=%async_computation | async-start | bytes 4194304 | tf_op jit(solution)/shard_map/all_to_all | solution.py:319
  89.2 1.2 copy-start.1
  91.8 36.0 %collective-permute-start.1 = (bf16[4,128,2048]{2,1,0:T(8,128)(2,1)S(1)}, bf16[4,128,2048]{2,1,0:T(8,128)(2,1)}, u32[]{:S(2)}, u32[]{:S(2)}) collective-permute-start(bf16[4,128,2048]{2,1,0:T(8,128)(2,1)S(1)} %all-to-all-done), channel_id=1, source_target_pairs={{0,1},{1,0},{2,3},{3,2},{4,5},{5,4},{6,7},{7,6},{8,9},{9,8},{10,11... | collective-permute-start | bytes 6291464 | tf_op jit(solution)/shard_map/ppermute | solution.py:26
  105.0 42.4 %all-to-all-start.1 = ((bf16[4,16,32,768]{3,2,1,0:T(8,128)(2,1)}), bf16[4,16,32,768]{3,2,1,0:T(8,128)(2,1)}, u32[]{:S(2)}, u32[]{:S(2)}) async-start(bf16[4,16,32,768]{3,2,1,0:T(8,128)(2,1)} %broadcast_in_dim.10), calls=%async_computation.1 | async-start | bytes 6291456 | tf_op jit(solution)/shard_map/all_to_all | solution.py:324
  123.0 4.8 %collective-permute-start = (bf16[4,256,128]{2,1,0:T(8,128)(2,1)S(1)}, bf16[4,256,128]{2,1,0:T(8,128)(2,1)S(1)}, u32[]{:S(2)}, u32[]{:S(2)}) collective-permute-start(bf16[4,256,128]{2,1,0:T(8,128)(2,1)S(1)} %bitcast.42), channel_id=1, source_target_pairs={{0,1},{1,0},{2,3},{3,2},{4,5},{5,4},{6,7},{7,6},{8,9},{9,8},{10,11... | collective-permute-start | bytes 786440 | tf_op jit(solution)/shard_map/ppermute | solution.py:26
  126.7 1.2 copy-start.3
  127.4 20.1 %copy-start = (f32[2048]{0:T(1024)S(1)}, f32[2048]{0:T(1024)}, u32[]{:S(2)}) copy-start(f32[2048]{0:T(1024)} %param.22) | copy-start | bytes 24580
  154.5 4.3 %collective-permute-start.2 = (bf16[4,32,2048]{2,1,0:T(8,128)(2,1)S(1)}, bf16[4,32,2048]{2,1,0:T(8,128)(2,1)S(1)}, u32[]{:S(2)}, u32[]{:S(2)}) collective-permute-start(bf16[4,32,2048]{2,1,0:T(8,128)(2,1)S(1)} %get-tuple-element.24), channel_id=1, source_target_pairs={{0,1},{1,0},{2,3},{3,2},{4,5},{5,4},{6,7},{7,6},{8,9},{9,8},{10,11... | collective-permute-start | bytes 1572872 | tf_op jit(solution)/shard_map/ppermute | solution.py:26
  180.5 6.1 %collective-permute-start.3 = (bf16[4,32,2048]{2,1,0:T(8,128)(2,1)S(1)}, bf16[4,32,2048]{2,1,0:T(8,128)(2,1)S(1)}, u32[]{:S(2)}, u32[]{:S(2)}) collective-permute-start(bf16[4,32,2048]{2,1,0:T(8,128)(2,1)S(1)} %all_to_all.21), channel_id=1, source_target_pairs={{0,1},{1,0},{2,3},{3,2},{4,5},{5,4},{6,7},{7,6},{8,9},{9,8},{10,11... | collective-permute-start | bytes 1572872 | tf_op jit(solution)/shard_map/ppermute | solution.py:26
Sparse Core Ops, SparseCore 0:
  22.1 99.7 all-gather.5
